TPU v7x, 32 devices: a whole 2x2x4 slice. The times are simulated.
32 devices in a mesh: ep: 32 (over z, y, x, core).
Axes of the slice: x: 2, y: 2, z: 4, core: 2. Of those that a mesh axis runs over, the one named last changes fastest.
Arguments:
- tokens: bfloat16 [128, 2048], P('ep'), may hold values from -6 to 6
- recurrent_state: float32 [128, 8, 128, 128], P('ep'), may hold values from -4 to 4
- query_weight: bfloat16 [2048, 1024], P(None, 'ep'), may hold values from -0.125 to 0.125
- forget_weight: bfloat16 [2048, 1024], P(None, 'ep'), may hold values from -0.125 to 0.125
- input_weight: bfloat16 [2048, 1024], P(None, 'ep'), may hold values from -0.125 to 0.125
- outgate_weight: bfloat16 [2048, 1024], P(None, 'ep'), may hold values from -0.125 to 0.125
- lower_bound: float32 [1024], replicated, may hold values from 0 to 0.9
- head_gain: float32 [128], replicated, may hold values from 0.1 to 1.9
- mixout_weight: bfloat16 [1024, 2048], P(None, 'ep'), may hold values from -0.1875 to 0.1875
- first_gain: float32 [2048], replicated, may hold values from 0.1 to 1.9
- first_bias: float32 [2048], replicated, may hold values from -1.5 to 1.5
- router_weight: bfloat16 [2048, 8], replicated, may hold values from -0.125 to 0.125
- branch_vector: bfloat16 [2048], replicated, may hold values from -0.125 to 0.125
- dense_gate_weight: bfloat16 [2048, 5632], P(None, 'ep'), may hold values from -0.125 to 0.125
- dense_up_weight: bfloat16 [2048, 5632], P(None, 'ep'), may hold values from -0.125 to 0.125
- dense_down_weight: bfloat16 [5632, 2048], P('ep'), may hold values from -0.078125 to 0.078125
- expert_gate_weight: bfloat16 [2048, 57344], P(None, 'ep'), may hold values from -0.125 to 0.125
- expert_up_weight: bfloat16 [2048, 57344], P(None, 'ep'), may hold values from -0.125 to 0.125
- expert_down_weight: bfloat16 [57344, 2048], P('ep'), may hold values from -0.0625 to 0.0625
- second_gain: float32 [2048], replicated, may hold values from 0.1 to 1.9
- second_bias: float32 [2048], replicated, may hold values from -1.5 to 1.5
- routes: int32 [128, 2], replicated, may hold values from 0 to 7, all different within a row; in each aligned block of 4 rows (0 to 3, 4 to 7, ...) at most 2 rows name the same one
Outputs:
- output: bfloat16 [128, 2048], P('ep')
- new_state: float32 [128, 8, 128, 128], P('ep')
Inputs may be any that keep to these rules, and one draw needn't show every extreme that they name: `routes`: each row names two different experts; in the rows of one device no expert is named more than 2 times, a bound that some block reaches in some device's rows.
All inputs are finite; a program needn't handle non-finite values.
Results may differ from a plain program's by a relative error of at most 0.0095.
Values may be sent and summed in bfloat16 or wider, within the bound.
A program may use at most 64 MiB of HBM per device.

v0:
```python
import jax
import jax.numpy as jnp
from jax import lax
from jax.sharding import PartitionSpec as P

EXPERTS = 8
CAP = 2


ALPHA = 8.0**0.25
NORM_EPS = 1e-05
HEAD_EPS = 1e-06


def layer_norm(mixture, gain, bias):
    center = jnp.mean(mixture, axis=-1, keepdims=True)
    spread = jnp.mean(jnp.square(mixture - center), axis=-1, keepdims=True)
    return (mixture - center) * lax.rsqrt(spread + NORM_EPS) * gain + bias


def recurrence(projected, state, lower_bound, head_gain):
    nseq, heads, width = (state.shape[0], state.shape[1], state.shape[2])
    query = projected[:, 0].astype(jnp.float32).reshape(nseq, heads, width)
    forget_in = projected[:, 1].astype(jnp.float32)
    value = projected[:, 2].astype(jnp.float32).reshape(nseq, heads, width)
    outgate = projected[:, 3].astype(jnp.float32)
    forget = (lower_bound + (1.0 - lower_bound) * jax.nn.sigmoid(forget_in)).reshape(
        nseq, heads, width
    )
    keyed = ((1.0 - lower_bound) * jax.nn.sigmoid(-forget_in)).reshape(nseq, heads, width)
    fresh = forget[..., None] * state + keyed[..., None] * value[:, :, None, :]
    read = jnp.einsum("bhkv,bhk->bhv", fresh, query, precision=lax.Precision.HIGHEST)
    scaled = (
        read * lax.rsqrt(jnp.mean(jnp.square(read), axis=-1, keepdims=True) + HEAD_EPS) * head_gain
    )
    mixed = (scaled.reshape(nseq, heads * width) * jax.nn.silu(outgate)).astype(jnp.bfloat16)
    return (mixed, fresh)


def route_share(rows, picks, router_weight):
    f32 = jnp.float32
    logits = jnp.dot(rows, router_weight, preferred_element_type=f32)
    expert_ids = jnp.arange(EXPERTS, dtype=jnp.int32)
    first_logit = jnp.sum(jnp.where(picks[:, 0:1] == expert_ids[None, :], logits, 0.0), axis=1)
    second_logit = jnp.sum(jnp.where(picks[:, 1:2] == expert_ids[None, :], logits, 0.0), axis=1)
    return jax.nn.sigmoid(first_logit - second_logit)


def channel_term(
    with_experts,
    normed_all,
    routes,
    start,
    count,
    router_weight,
    branch_vector,
    dense_gate_weight,
    dense_up_weight,
    dense_down_weight,
    expert_gate_weight,
    expert_up_weight,
    expert_down_weight,
):
    f32 = jnp.float32
    branch_gate = jax.nn.sigmoid(jnp.dot(normed_all, branch_vector, preferred_element_type=f32))
    dense_hidden = (
        jax.nn.silu(jnp.dot(normed_all, dense_gate_weight, preferred_element_type=f32))
        * jnp.dot(normed_all, dense_up_weight, preferred_element_type=f32)
    ).astype(jnp.bfloat16)
    dense_part = branch_gate[:, None] * jnp.dot(
        dense_hidden, dense_down_weight, preferred_element_type=f32
    )
    return dense_part


def expert_slots(
    own_rows, own_picks, router_weight, expert_gate_weight, expert_up_weight, expert_down_weight
):
    f32 = jnp.float32
    width = own_rows.shape[1]
    share = route_share(own_rows, own_picks, router_weight)
    expert_ids = jnp.arange(EXPERTS, dtype=jnp.int32)
    on_first = own_picks[None, :, 0] == expert_ids[:, None]
    on_second = own_picks[None, :, 1] == expert_ids[:, None]
    token_weight = share[None, :] * on_first.astype(f32) + (1.0 - share)[
        None, :
    ] * on_second.astype(f32)
    hits = (on_first | on_second).astype(jnp.int32)
    ranks = jnp.cumsum(hits, axis=1) - 1
    slot_ids = jnp.arange(CAP, dtype=jnp.int32)
    select = (ranks[:, None, :] == slot_ids[None, :, None]) & (hits[:, None, :] > 0)
    slot_rows = jnp.einsum(
        "eci,id->ecd", select.astype(jnp.bfloat16), own_rows, preferred_element_type=f32
    ).astype(jnp.bfloat16)
    spread_count = lax.axis_size("ep") // EXPERTS
    sent = jnp.repeat(slot_rows, spread_count, axis=0)
    arrived = lax.all_to_all(sent, "ep", split_axis=0, concat_axis=0, tiled=True)
    flat = arrived.reshape(-1, width)
    gate_part = jnp.dot(flat, expert_gate_weight, preferred_element_type=f32)
    up_part = jnp.dot(flat, expert_up_weight, preferred_element_type=f32)
    hidden = (jax.nn.silu(gate_part) * up_part).astype(jnp.bfloat16)
    made = jnp.dot(hidden, expert_down_weight, preferred_element_type=f32).reshape(arrived.shape)
    returned = lax.all_to_all(
        made.astype(jnp.bfloat16), "ep", split_axis=0, concat_axis=0, tiled=True
    ).astype(made.dtype)
    summed = jnp.sum(returned.reshape(EXPERTS, spread_count, CAP, width), axis=1)
    back = jnp.einsum("eci,ecd->eid", select.astype(f32), summed, precision=lax.Precision.HIGHEST)
    return jnp.sum(back * token_weight[:, :, None], axis=0)


def per_device(
    tokens,
    recurrent_state,
    query_weight,
    forget_weight,
    input_weight,
    outgate_weight,
    lower_bound,
    head_gain,
    mixout_weight,
    first_gain,
    first_bias,
    router_weight,
    branch_vector,
    dense_gate_weight,
    dense_up_weight,
    dense_down_weight,
    expert_gate_weight,
    expert_up_weight,
    expert_down_weight,
    second_gain,
    second_bias,
    routes,
):
    f32 = jnp.float32
    devices = lax.axis_size("ep")
    nseq, width = tokens.shape
    own_cols = query_weight.shape[1]
    row_start = lax.axis_index("ep") * nseq
    own_picks = lax.dynamic_slice_in_dim(routes, row_start, nseq, 0)
    stacked = jnp.concatenate([query_weight, forget_weight, input_weight, outgate_weight], axis=1)
    weights = (
        router_weight,
        branch_vector,
        dense_gate_weight,
        dense_up_weight,
        dense_down_weight,
        expert_gate_weight,
        expert_up_weight,
        expert_down_weight,
    )
    gathered = jnp.dot(
        lax.all_gather(tokens, "ep", axis=0, tiled=True), stacked, preferred_element_type=f32
    ).astype(jnp.bfloat16)
    owned = lax.all_to_all(gathered, "ep", split_axis=0, concat_axis=1, tiled=True)
    projected = (
        owned.reshape(nseq, devices, 4, own_cols)
        .transpose(0, 2, 1, 3)
        .reshape(nseq, 4, devices * own_cols)
    )
    mixed, new_state = recurrence(projected, recurrent_state, lower_bound, head_gain)
    mix_cols = jnp.dot(
        lax.all_gather(mixed, "ep", axis=0, tiled=True), mixout_weight, preferred_element_type=f32
    ).astype(jnp.bfloat16)
    mix_out = lax.all_to_all(mix_cols, "ep", split_axis=0, concat_axis=1, tiled=True)
    normed = layer_norm(
        ALPHA * tokens.astype(f32) + mix_out.astype(f32), first_gain, first_bias
    ).astype(jnp.bfloat16)
    normed_all = lax.all_gather(normed, "ep", axis=0, tiled=True)
    channel = lax.psum_scatter(
        channel_term(False, normed_all, routes, jnp.int32(0), nseq * lax.axis_size("ep"), *weights),
        "ep",
        scatter_dimension=0,
        tiled=True,
    )
    channel = channel + expert_slots(
        normed, own_picks, router_weight, expert_gate_weight, expert_up_weight, expert_down_weight
    )
    output = layer_norm(ALPHA * normed.astype(f32) + channel, second_gain, second_bias).astype(
        jnp.bfloat16
    )
    return (output, new_state)


def solution(mesh):
    return jax.shard_map(
        per_device,
        mesh=mesh,
        in_specs=(
            P("ep", None),
            P("ep", None, None, None),
            P(None, "ep"),
            P(None, "ep"),
            P(None, "ep"),
            P(None, "ep"),
            P(),
            P(),
            P(None, "ep"),
            P(),
            P(),
            P(),
            P(),
            P(None, "ep"),
            P(None, "ep"),
            P("ep", None),
            P(None, "ep"),
            P(None, "ep"),
            P("ep", None),
            P(),
            P(),
            P(),
        ),
        out_specs=(P("ep", None), P("ep", None, None, None)),
        check_vma=False,
    )
```

profile of v0, /device:TPU:29, one launch (start us, length us, event | category | flops | bytes accessed | tf_op | source)
XLA Modules:
  0.0 308.3 jit_solution(12458948402277351714)
XLA Ops:
  7.2 37.6 %all-gather = bf16[32,4,2048]{2,1,0:T(4,128)(2,1)S(1)} all-gather(bf16[1,4,2048]{2,1,0:T(4,128)(2,1)} %bitcast.89), channel_id=1, replica_groups=mesh['ep'=32] {'ep'}, dimensions={0}, use_global_device_ids=true | all-gather | bytes 540672 | tf_op jit(solution)/shard_map/all_gather | solution.py:153
  44.9 2.0 convolution_convert_fusion.2
  47.0 8.9 %all-to-all-start = ((bf16[32,4,128]{2,1,0:T(4,128)(2,1)}), bf16[32,4,128]{2,1,0:T(4,128)(2,1)S(1)}, u32[]{:S(2)}, u32[]{:S(2)}) async-start(bf16[32,4,128]{2,1,0:T(4,128)(2,1)} %bitcast.4), calls=%async_computation | async-start | bytes 65536 | tf_op jit(solution)/shard_map/all_to_all | solution.py:155
  57.9 1.1 all-to-all-done
  60.2 2.5 multiply_add_fusion
  62.7 1.1 fusion.28
  63.9 36.5 %all-gather.1 = bf16[32,4,1024]{2,1,0:T(4,128)(2,1)S(1)} all-gather(bf16[1,4,1024]{2,1,0:T(4,128)(2,1)S(1)} %fusion.34), channel_id=1, replica_groups=mesh['ep'=32] {'ep'}, dimensions={0}, use_global_device_ids=true | all-gather | bytes 270336 | tf_op jit(solution)/shard_map/all_gather | solution.py:163
  101.6 7.7 %all-to-all-start.1 = ((bf16[32,2,128]{2,1,0:T(2,128)(2,1)}), bf16[32,2,128]{2,1,0:T(2,128)(2,1)S(1)}, u32[]{:S(2)}, u32[]{:S(2)}) async-start(bf16[32,2,128]{2,1,0:T(2,128)(2,1)} %reshape.327), calls=%async_computation.1 | async-start | bytes 32768 | tf_op jit(solution)/shard_map/all_to_all | solution.py:165
  109.3 2.7 all-to-all-done.1
  112.7 40.2 %all-gather.2 = bf16[32,4,2048]{2,1,0:T(4,128)(2,1)} all-gather(bf16[1,4,2048]{2,1,0:T(4,128)(2,1)S(1)} %bitcast.90), channel_id=1, replica_groups=mesh['ep'=32] {'ep'}, dimensions={0}, use_global_device_ids=true | all-gather | bytes 540672 | tf_op jit(solution)/shard_map/all_gather | solution.py:169
  152.9 1.2 reshape.320
  155.1 8.3 %all-to-all-start.2 = ((bf16[32,2,2048]{2,1,0:T(2,128)(2,1)}), bf16[32,2,2048]{2,1,0:T(2,128)(2,1)}, u32[]{:S(2)}, u32[]{:S(2)}) async-start(bf16[32,2,2048]{2,1,0:T(2,128)(2,1)} %bitcast.87), calls=%async_computation.2 | async-start | bytes 524288 | tf_op jit(solution)/shard_map/all_to_all | solution.py:97
  163.5 1.5 fusion.43
  165.2 3.1 %convolution_multiply_fusion = f32[128,2048]{1,0:T(8,128)} fusion(bf16[176,2048]{1,0:T(8,128)(2,1)S(1)} %copy-done, bf16[128,2048]{1,0:T(8,128)(2,1)S(1)} %reshape.320, bf16[2048,176]{0,1:T(8,128)(2,1)} %param.36, f32[128]{0:T(128)S(1)} %fusion.6, f32[128,176]{0,1:T(8,128)S(1)} %fusion.43), kind=kOutput, calls=%fused_computation | convolution fusion | flops 184946688 | bytes 3105280 | tf_op jit(solution)/shard_map/dot_general | solution.py:70
  168.3 2.2 all-to-all-done.2
  170.5 1.0 reshape.305
  171.6 4.4 %fusion.44 = f32[64,1792]{1,0:T(8,128)S(1)} fusion(bf16[64,2048]{1,0:T(8,128)(2,1)S(1)} %reshape.305, bf16[2048,1792]{1,0:T(8,128)(2,1)} %param.38), kind=kOutput, calls=%fused_computation.94 | convolution fusion | flops 469762048 | bytes 8060928 | tf_op jit(solution)/shard_map/dot_general | solution.py:99
  176.0 8.7 %convolution_convert_fusion = bf16[64,2048]{1,0:T(8,128)(2,1)} fusion(bf16[1792,2048]{1,0:T(8,128)(2,1)} %param.40, bf16[64,2048]{1,0:T(8,128)(2,1)S(1)} %reshape.305, bf16[2048,1792]{1,0:T(8,128)(2,1)} %param.39, f32[64,1792]{1,0:T(8,128)S(1)} %fusion.44), kind=kOutput, calls=%fused_computation.3 | convolution fusion | flops 940343296 | bytes 15663104 | tf_op jit(solution)/shard_map/dot_general | solution.py:102
  184.7 1.9 convert_element_type.112
  186.6 6.2 %all-to-all-start.3 = ((bf16[32,2,2048]{2,1,0:T(2,128)(2,1)}), bf16[32,2,2048]{2,1,0:T(2,128)(2,1)S(1)}, u32[]{:S(2)}, u32[]{:S(2)}) async-start(bf16[32,2,2048]{2,1,0:T(2,128)(2,1)} %convert_element_type.112), calls=%async_computation.3 | async-start | bytes 524288 | tf_op jit(solution)/shard_map/all_to_all | solution.py:103
  194.6 6.5 %all-to-all-done.3 = bf16[32,2,2048]{2,1,0:T(2,128)(2,1)S(1)} async-done(((bf16[32,2,2048]{2,1,0:T(2,128)(2,1)}), bf16[32,2,2048]{2,1,0:T(2,128)(2,1)S(1)}, u32[]{:S(2)}, u32[]{:S(2)}) %all-to-all-start.3) | async-done | bytes 262176 | tf_op jit(solution)/shard_map/all_to_all | solution.py:103
  201.3 1.1 fusion.1
  202.4 96.5 %all-reduce.3.cloned.1.call-done = f32[128,2048]{1,0:T(8,128)} async-done(((f32[128,2048]{1,0:T(8,128)}), f32[128,2048]{1,0:T(8,128)}) %all-reduce.3.cloned.1.call-update) | async-done | bytes 1048592
  300.1 1.4 add_convert_fusion
  (69 shorter events, 9.9 us)
Async XLA Ops:
  7.2 158.0 %copy-start = (bf16[176,2048]{1,0:T(8,128)(2,1)S(1)}, bf16[176,2048]{1,0:T(8,128)(2,1)}, u32[]{:S(2)}) copy-start(bf16[176,2048]{1,0:T(8,128)(2,1)} %param.37) | copy-start | bytes 2162692
  7.2 105.1 %copy-start.2 = (bf16[4,2048]{1,0:T(4,128)(2,1)S(1)}, bf16[4,2048]{1,0:T(4,128)(2,1)}, u32[]{:S(2)}) copy-start(bf16[4,2048]{1,0:T(4,128)(2,1)} %param.22) | copy-start | bytes 49156
  7.2 56.6 %copy-start.10 = (f32[128]{0:T(128)S(1)}, f32[128]{0:T(128)}, u32[]{:S(2)}) copy-start(f32[128]{0:T(128)} %param.29) | copy-start | bytes 1540
  7.2 93.3 %copy-start.3 = (bf16[1024,64]{0,1:T(8,128)(2,1)S(1)}, bf16[1024,64]{0,1:T(8,128)(2,1)}, u32[]{:S(2)}) copy-start(bf16[1024,64]{0,1:T(8,128)(2,1)} %param.30) | copy-start | bytes 393220
  7.2 102.1 %copy-start.9 = (bf16[2048]{0:T(1024)(128)(2,1)S(1)}, bf16[2048]{0:T(1024)(128)(2,1)}, u32[]{:S(2)}) copy-start(bf16[2048]{0:T(1024)(128)(2,1)} %param.34) | copy-start | bytes 12292
  7.2 105.4 %copy-start.6 = (f32[2048]{0:T(1024)S(1)}, f32[2048]{0:T(1024)}, u32[]{:S(2)}) copy-start(f32[2048]{0:T(1024)} %param.31) | copy-start | bytes 24580
  7.2 105.4 %copy-start.5 = (f32[2048]{0:T(1024)S(1)}, f32[2048]{0:T(1024)}, u32[]{:S(2)}) copy-start(f32[2048]{0:T(1024)} %param.32) | copy-start | bytes 24580
  47.0 12.1 %all-to-all-start = ((bf16[32,4,128]{2,1,0:T(4,128)(2,1)}), bf16[32,4,128]{2,1,0:T(4,128)(2,1)S(1)}, u32[]{:S(2)}, u32[]{:S(2)}) async-start(bf16[32,4,128]{2,1,0:T(4,128)(2,1)} %bitcast.4), calls=%async_computation | async-start | bytes 65536 | tf_op jit(solution)/shard_map/all_to_all | solution.py:155
  57.3 0.5 copy-start.7
  57.3 52.0 %copy-start.8 = (s32[4]{0:T(128)}, s32[4]{0:T(128)S(1)}, u32[]{:S(2)}) copy-start(s32[4]{0:T(128)S(1)} %get-tuple-element.17) | copy-start | bytes 52
  62.6 113.4 %copy-start.1 = (f32[4,8,128,128]{3,2,1,0:T(8,128)}, f32[4,8,128,128]{3,2,1,0:T(8,128)S(1)}, u32[]{:S(2)}) copy-start(f32[4,8,128,128]{3,2,1,0:T(8,128)S(1)} %multiply_add_fusion) | copy-start | bytes 6291460
  101.6 10.5 %all-to-all-start.1 = ((bf16[32,2,128]{2,1,0:T(2,128)(2,1)}), bf16[32,2,128]{2,1,0:T(2,128)(2,1)S(1)}, u32[]{:S(2)}, u32[]{:S(2)}) async-start(bf16[32,2,128]{2,1,0:T(2,128)(2,1)} %reshape.327), calls=%async_computation.1 | async-start | bytes 32768 | tf_op jit(solution)/shard_map/all_to_all | solution.py:165
  109.3 61.3 %copy-start.4 = (pred[8,2,4]{2,1,0:T(4,128)(4,1)}, pred[8,2,4]{2,1,0:T(4,128)(4,1)S(1)}, u32[]{:S(2)}) copy-start(pred[8,2,4]{2,1,0:T(4,128)(4,1)S(1)} %compare_and_fusion) | copy-start | bytes 196
  155.1 15.4 %all-to-all-start.2 = ((bf16[32,2,2048]{2,1,0:T(2,128)(2,1)}), bf16[32,2,2048]{2,1,0:T(2,128)(2,1)}, u32[]{:S(2)}, u32[]{:S(2)}) async-start(bf16[32,2,2048]{2,1,0:T(2,128)(2,1)} %bitcast.87), calls=%async_computation.2 | async-start | bytes 524288 | tf_op jit(solution)/shard_map/all_to_all | solution.py:97
  163.4 135.5 %all-reduce.3.cloned.1.call-start = ((), (), s32[]{:S(2)}) async-start(), calls=%async_computation.4 | async-start | bytes 2097152
  186.6 14.5 %all-to-all-start.3 = ((bf16[32,2,2048]{2,1,0:T(2,128)(2,1)}), bf16[32,2,2048]{2,1,0:T(2,128)(2,1)S(1)}, u32[]{:S(2)}, u32[]{:S(2)}) async-start(bf16[32,2,2048]{2,1,0:T(2,128)(2,1)} %convert_element_type.112), calls=%async_computation.3 | async-start | bytes 524288 | tf_op jit(solution)/shard_map/all_to_all | solution.py:103
Sparse Core Ops, SparseCore 0:
  169.4 129.4 all-reduce.2
where the time goes:
time: 314 us; the launch traced here: 308 us
  blocking collectives  114 us (36%)
  waiting for transfers between devices  109 us (35%)
  starting transfers between devices  31.1 us (10%)
  matrix products  23.5 us (7%)
  between operations  14.4 us (5%)
  other arithmetic  8.33 us (3%)
  local copies, waits for them, and re-layouts  7.81 us (2%)
    unnamed x2, waiting for transfers between devices  96.5 us
    all_gather x1, blocking collectives, per_device(): normed_all = lax.all_gather(normed, 'ep', axis=0, tiled=True)  40.2 us
    all_gather x1, blocking collectives, per_device(): lax.all_gather(tokens, 'ep', axis=0, tiled=True)  37.6 us
    all_gather x1, blocking collectives, per_device(): lax.all_gather(mixed, 'ep', axis=0, tiled=True)  36.5 us
    all_to_all x1, starting transfers between devices, per_device(): lax.all_to_all(gathered, 'ep', split_axis=0, concat_axis=1, tiled=True)  8.86 us
    dot_general x1, matrix products, expert_slots(): jnp.dot(hidden, expert_down_weight, preferred_element_type=f32)  8.67 us
    all_to_all x1, starting transfers between devices, expert_slots(): lax.all_to_all(sent, 'ep', split_axis=0, concat_axis=0, tiled=True)  8.28 us
    all_to_all x1, starting transfers between devices, per_device(): lax.all_to_all(mix_cols, 'ep', split_axis=0, concat_axis=1, tiled=True)  7.68 us
  transfers between devices with their start and end apart: 5, of which 5 were waited for; matrix products, arithmetic and copies ran while one was open for 8% of the time, Pallas kernels for 0%

commit v1 on v0

v1 whole, which is shorter than its diff:
```python
import jax
import jax.numpy as jnp
from jax import lax
from jax.sharding import PartitionSpec as P

EXPERTS = 8


ALPHA = 8.0**0.25
NORM_EPS = 1e-05
HEAD_EPS = 1e-06


def layer_norm(mixture, gain, bias):
    center = jnp.mean(mixture, axis=-1, keepdims=True)
    spread = jnp.mean(jnp.square(mixture - center), axis=-1, keepdims=True)
    return (mixture - center) * lax.rsqrt(spread + NORM_EPS) * gain + bias


def recurrence(projected, state, lower_bound, head_gain):
    nseq, heads, width = (state.shape[0], state.shape[1], state.shape[2])
    query = projected[:, 0].astype(jnp.float32).reshape(nseq, heads, width)
    forget_in = projected[:, 1].astype(jnp.float32)
    value = projected[:, 2].astype(jnp.float32).reshape(nseq, heads, width)
    outgate = projected[:, 3].astype(jnp.float32)
    forget = (lower_bound + (1.0 - lower_bound) * jax.nn.sigmoid(forget_in)).reshape(
        nseq, heads, width
    )
    keyed = ((1.0 - lower_bound) * jax.nn.sigmoid(-forget_in)).reshape(nseq, heads, width)
    fresh = forget[..., None] * state + keyed[..., None] * value[:, :, None, :]
    read = jnp.einsum("bhkv,bhk->bhv", fresh, query, precision=lax.Precision.HIGHEST)
    scaled = (
        read * lax.rsqrt(jnp.mean(jnp.square(read), axis=-1, keepdims=True) + HEAD_EPS) * head_gain
    )
    mixed = (scaled.reshape(nseq, heads * width) * jax.nn.silu(outgate)).astype(jnp.bfloat16)
    return (mixed, fresh)


def route_share(rows, picks, router_weight):
    f32 = jnp.float32
    logits = jnp.dot(rows, router_weight, preferred_element_type=f32)
    expert_ids = jnp.arange(EXPERTS, dtype=jnp.int32)
    first_logit = jnp.sum(jnp.where(picks[:, 0:1] == expert_ids[None, :], logits, 0.0), axis=1)
    second_logit = jnp.sum(jnp.where(picks[:, 1:2] == expert_ids[None, :], logits, 0.0), axis=1)
    return jax.nn.sigmoid(first_logit - second_logit)


def spread(block):
    count = lax.axis_size("ep")
    copies = jnp.broadcast_to(block[None], (count,) + block.shape)
    arrived = lax.all_to_all(copies, "ep", split_axis=0, concat_axis=0, tiled=True)
    return arrived.reshape(count * block.shape[0], block.shape[1])


def channel_partial(
    rows,
    routes,
    router_weight,
    branch_vector,
    dense_gate_weight,
    dense_up_weight,
    dense_down_weight,
    expert_gate_weight,
    expert_up_weight,
    expert_down_weight,
):
    f32 = jnp.float32
    share = route_share(rows, routes, router_weight)
    expert = lax.axis_index("ep") // (lax.axis_size("ep") // EXPERTS)
    on_first = routes[:, 0] == expert
    on_second = routes[:, 1] == expert
    weight = jnp.where(on_first, share, jnp.where(on_second, 1.0 - share, 0.0))
    branch_gate = jax.nn.sigmoid(jnp.dot(rows, branch_vector, preferred_element_type=f32))

    def ffn(gate_weight, up_weight, down_weight):
        gate_part = jnp.dot(rows, gate_weight, preferred_element_type=f32)
        up_part = jnp.dot(rows, up_weight, preferred_element_type=f32)
        hidden = (jax.nn.silu(gate_part) * up_part).astype(jnp.bfloat16)
        return jnp.dot(hidden, down_weight, preferred_element_type=f32)

    dense = ffn(dense_gate_weight, dense_up_weight, dense_down_weight)
    routed = ffn(expert_gate_weight, expert_up_weight, expert_down_weight)
    picked = (on_first | on_second)[:, None]
    return branch_gate[:, None] * dense + jnp.where(picked, weight[:, None] * routed, 0.0)


def per_device(
    tokens,
    recurrent_state,
    query_weight,
    forget_weight,
    input_weight,
    outgate_weight,
    lower_bound,
    head_gain,
    mixout_weight,
    first_gain,
    first_bias,
    router_weight,
    branch_vector,
    dense_gate_weight,
    dense_up_weight,
    dense_down_weight,
    expert_gate_weight,
    expert_up_weight,
    expert_down_weight,
    second_gain,
    second_bias,
    routes,
):
    f32 = jnp.float32
    devices = lax.axis_size("ep")
    nseq, width = tokens.shape
    own_cols = query_weight.shape[1]
    stacked = jnp.concatenate([query_weight, forget_weight, input_weight, outgate_weight], axis=1)
    weights = (
        router_weight,
        branch_vector,
        dense_gate_weight,
        dense_up_weight,
        dense_down_weight,
        expert_gate_weight,
        expert_up_weight,
        expert_down_weight,
    )
    gathered = jnp.dot(
        spread(tokens), stacked, preferred_element_type=f32
    ).astype(jnp.bfloat16)
    owned = lax.all_to_all(gathered, "ep", split_axis=0, concat_axis=1, tiled=True)
    projected = (
        owned.reshape(nseq, devices, 4, own_cols)
        .transpose(0, 2, 1, 3)
        .reshape(nseq, 4, devices * own_cols)
    )
    mixed, new_state = recurrence(projected, recurrent_state, lower_bound, head_gain)
    mix_cols = jnp.dot(
        spread(mixed), mixout_weight, preferred_element_type=f32
    ).astype(jnp.bfloat16)
    mix_out = lax.all_to_all(mix_cols, "ep", split_axis=0, concat_axis=1, tiled=True)
    normed = layer_norm(
        ALPHA * tokens.astype(f32) + mix_out.astype(f32), first_gain, first_bias
    ).astype(jnp.bfloat16)
    partial = channel_partial(spread(normed), routes, *weights).astype(jnp.bfloat16)
    arrived = lax.all_to_all(
        partial.reshape(devices, nseq, width), "ep", split_axis=0, concat_axis=0, tiled=True
    )
    channel = jnp.sum(arrived.astype(f32), axis=0)
    output = layer_norm(ALPHA * normed.astype(f32) + channel, second_gain, second_bias).astype(
        jnp.bfloat16
    )
    return (output, new_state)


def solution(mesh):
    return jax.shard_map(
        per_device,
        mesh=mesh,
        in_specs=(
            P("ep", None),
            P("ep", None, None, None),
            P(None, "ep"),
            P(None, "ep"),
            P(None, "ep"),
            P(None, "ep"),
            P(),
            P(),
            P(None, "ep"),
            P(),
            P(),
            P(),
            P(),
            P(None, "ep"),
            P(None, "ep"),
            P("ep", None),
            P(None, "ep"),
            P(None, "ep"),
            P("ep", None),
            P(),
            P(),
            P(),
        ),
        out_specs=(P("ep", None), P("ep", None, None, None)),
        check_vma=False,
    )
```

time: 314 us -> 122 us (0.39)
  the two profiles are of different devices: /device:TPU:29 before, /device:TPU:0 now
where the time goes in v1:
time: 122 us
  blocking collectives  62.6 us (51%)
  waiting for transfers between devices  22.1 us (18%)
  matrix products  19.4 us (16%)
  starting transfers between devices  6.31 us (5%)
  other arithmetic  5.9 us (5%)
  local copies, waits for them, and re-layouts  4.45 us (4%)
    all_to_all x2, blocking collectives, spread(): lax.all_to_all(copies, 'ep', split_axis=0, concat_axis=0, tiled=True)  35 us
    all_to_all x1, blocking collectives, per_device(): lax.all_to_all(partial.reshape(devices, nseq, width), 'ep', split_axis=0,...  18.3 us
    all_to_all x1, waiting for transfers between devices, spread(): lax.all_to_all(copies, 'ep', split_axis=0, concat_axis=0, tiled=True)  15.5 us
    dot_general x2, matrix products, ffn(): return jnp.dot(hidden, down_weight, preferred_element_type=f32)  10 us
    all_to_all x1, blocking collectives, per_device(): lax.all_to_all(mix_cols, 'ep', split_axis=0, concat_axis=1, tiled=True)  9.29 us
    all_to_all x1, waiting for transfers between devices, per_device(): lax.all_to_all(gathered, 'ep', split_axis=0, concat_axis=1, tiled=True)  6.56 us
    dot_general x2, matrix products, ffn(): gate_part = jnp.dot(rows, gate_weight, preferred_element_type=f32)  5.56 us
    all_to_all x1, starting transfers between devices, spread(): lax.all_to_all(copies, 'ep', split_axis=0, concat_axis=0, tiled=True)  3.33 us
  transfers between devices with their start and end apart: 2, of which 2 were waited for; matrix products, arithmetic and copies ran while one was open for 1% of the time, Pallas kernels for 0%

profile of v1, /device:TPU:0, one launch (start us, length us, event | category | flops | bytes accessed | tf_op | source)
XLA Modules:
  0.0 121.7 jit_solution(17449275505892142216)
XLA Ops:
  0.7 1.0 broadcast_in_dim.24
  1.7 22.7 %all_to_all.49 = bf16[32,4,2048]{2,1,0:T(4,128)(2,1)S(1)} all-to-all(bf16[32,4,2048]{2,1,0:T(4,128)(2,1)S(1)} %broadcast_in_dim.24), channel_id=1, replica_groups=mesh['ep'=32] {'ep'}, dimensions={0} | all-to-all | bytes 1048576 | tf_op jit(solution)/shard_map/all_to_all | solution.py:51
  24.6 2.0 %convolution_convert_fusion = bf16[128,128]{0,1:T(8,128)(2,1)} fusion(bf16[128,2048]{1,0:T(8,128)(2,1)S(1)} %reshape.190, bf16[2048,32]{0,1:T(8,128)(2,1)} %param.27, bf16[2048,32]{0,1:T(8,128)(2,1)} %param.26, bf16[2048,32]{0,1:T(8,128)(2,1)} %param.25, bf16[2048,32]{0,1:T(8,128)(2,1)} %param.24), kind=kOutput, calls=%fused_computation.10 | convolution fusion | flops 69222400 | bytes 1081344 | tf_op jit(solution)/shard_map/dot_general | solution.py:126
  26.6 3.0 %all-to-all-start.1 = ((bf16[32,4,128]{2,1,0:T(4,128)(2,1)}), bf16[32,4,128]{2,1,0:T(4,128)(2,1)S(1)}, u32[]{:S(2)}, u32[]{:S(2)}) async-start(bf16[32,4,128]{2,1,0:T(4,128)(2,1)} %bitcast.3), calls=%async_computation.1 | async-start | bytes 65536 | tf_op jit(solution)/shard_map/all_to_all | solution.py:129
  29.6 0.7 subtract_bitcast_fusion
  30.3 6.6 %all-to-all-done.1 = bf16[32,4,128]{2,1,0:T(4,128)(2,1)S(1)} async-done(((bf16[32,4,128]{2,1,0:T(4,128)(2,1)}), bf16[32,4,128]{2,1,0:T(4,128)(2,1)S(1)}, u32[]{:S(2)}, u32[]{:S(2)}) %all-to-all-start.1) | async-done | bytes 32800 | tf_op jit(solution)/shard_map/all_to_all | solution.py:129
  37.3 0.7 multiply_add_fusion.3
  38.0 2.5 %multiply_add_fusion = f32[4,8,128,128]{3,2,1,0:T(8,128)S(1)} fusion(f32[4,8,128,128]{3,2,1,0:T(8,128)} %param.23, f32[4,8,128]{2,1,0:T(8,128)S(1)} %bitcast.84, f32[4,8,128]{2,1,0:T(8,128)S(1)} %get-tuple-element.9, f32[4,8,128]{2,1,0:T(8,128)S(1)} %get-tuple-element.8), kind=kLoop, calls=%fused_computation.7 | loop fusion | flops 1572864 | bytes 4243456 | tf_op jit(solution)/shard_map/add | solution.py:30
  40.5 1.1 fusion.24
  41.8 12.3 %all_to_all.50 = bf16[32,4,1024]{2,1,0:T(4,128)(2,1)S(1)} all-to-all(bf16[32,4,1024]{2,1,0:T(4,128)(2,1)S(1)} %broadcast_in_dim.25), channel_id=1, replica_groups=mesh['ep'=32] {'ep'}, dimensions={0} | all-to-all | bytes 524288 | tf_op jit(solution)/shard_map/all_to_all | solution.py:51
  54.6 9.3 %all_to_all.51 = bf16[32,2,128]{2,1,0:T(2,128)(2,1)S(1)} all-to-all(bf16[32,2,128]{2,1,0:T(2,128)(2,1)S(1)} %reshape.210), channel_id=1, replica_groups=mesh['ep'=32] {'ep'}, dimensions={0} | all-to-all | bytes 32768 | tf_op jit(solution)/shard_map/all_to_all | solution.py:139
  64.6 1.0 broadcast_in_dim.27
  65.6 3.3 %all-to-all-start.4 = ((bf16[32,4,2048]{2,1,0:T(4,128)(2,1)}), bf16[32,4,2048]{2,1,0:T(4,128)(2,1)}, u32[]{:S(2)}, u32[]{:S(2)}) async-start(bf16[32,4,2048]{2,1,0:T(4,128)(2,1)} %broadcast_in_dim.27), calls=%async_computation.4 | async-start | bytes 1048576 | tf_op jit(solution)/shard_map/all_to_all | solution.py:51
  69.1 15.5 %all-to-all-done.4 = bf16[32,4,2048]{2,1,0:T(4,128)(2,1)} async-done(((bf16[32,4,2048]{2,1,0:T(4,128)(2,1)}), bf16[32,4,2048]{2,1,0:T(4,128)(2,1)}, u32[]{:S(2)}, u32[]{:S(2)}) %all-to-all-start.4) | async-done | bytes 524320 | tf_op jit(solution)/shard_map/all_to_all | solution.py:51
  84.6 1.2 reshape.196
  85.8 5.2 %fusion.35 = f32[128,1792]{1,0:T(8,128)} fusion(bf16[128,2048]{1,0:T(8,128)(2,1)S(1)} %reshape.196, bf16[2048,1792]{1,0:T(8,128)(2,1)} %param.38), kind=kOutput, calls=%fused_computation.79 | convolution fusion | flops 939524096 | bytes 8781824 | tf_op jit(solution)/shard_map/dot_general | solution.py:76
  91.0 0.4 fusion.34
  91.3 0.2 fusion.8
  91.6 0.3 select_reduce_fusion
  91.9 8.0 %fusion.1 = f32[128,2048]{1,0:T(8,128)S(1)} fusion(bf16[1792,2048]{1,0:T(8,128)(2,1)} %param.40, bf16[128,2048]{1,0:T(8,128)(2,1)S(1)} %reshape.196, bf16[2048,1792]{1,0:T(8,128)(2,1)} %param.39, f32[128,1792]{1,0:T(8,128)} %fusion.35, f32[128]{0:T(128)S(1)} %fusion.30, pred[128]{0:T(512)(128)(4,1)S(1)} %or_bitcast_fusion), kind=kOutput, calls=%fused_computation.4 | convolution fusion | flops 1880948736 | bytes 17171072 | tf_op jit(solution)/shard_map/dot_general | solution.py:79
  99.9 2.0 %fusion.3 = bf16[128,2048]{1,0:T(8,128)(2,1)S(1)} fusion(f32[128,2048]{1,0:T(8,128)S(1)} %fusion.1, bf16[176,2048]{1,0:T(8,128)(2,1)S(1)} %copy-done, bf16[128,2048]{1,0:T(8,128)(2,1)S(1)} %reshape.196, bf16[2048,176]{0,1:T(8,128)(2,1)} %param.36, f32[128]{0:T(128)S(1)} %fusion.8, f32[128,176]{0,1:T(8,128)S(1)} %fusion.34), kind=kOutput, calls=%fused_computation.6 | convolution fusion | flops 185470976 | bytes 3629568 | tf_op jit(solution)/shard_map/dot_general | solution.py:79
  102.2 18.3 %all_to_all.52 = bf16[32,4,2048]{2,1,0:T(4,128)(2,1)S(1)} all-to-all(bf16[32,4,2048]{2,1,0:T(4,128)(2,1)S(1)} %reshape.197), channel_id=1, replica_groups=mesh['ep'=32] {'ep'}, dimensions={0} | all-to-all | bytes 1048576 | tf_op jit(solution)/shard_map/all_to_all | solution.py:144
  120.4 0.2 convert_reduce_fusion
  121.0 0.7 add_convert_fusion
  (60 shorter events, 2.6 us)
Async XLA Ops:
  0.6 99.3 %copy-start = (bf16[176,2048]{1,0:T(8,128)(2,1)S(1)}, bf16[176,2048]{1,0:T(8,128)(2,1)}, u32[]{:S(2)}) copy-start(bf16[176,2048]{1,0:T(8,128)(2,1)} %param.37) | copy-start | bytes 2162692
  0.6 63.5 %copy-start.3 = (bf16[4,2048]{1,0:T(4,128)(2,1)S(1)}, bf16[4,2048]{1,0:T(4,128)(2,1)}, u32[]{:S(2)}) copy-start(bf16[4,2048]{1,0:T(4,128)(2,1)} %param.22) | copy-start | bytes 49156
  0.7 41.0 %copy-start.12 = (f32[128]{0:T(128)S(1)}, f32[128]{0:T(128)}, u32[]{:S(2)}) copy-start(f32[128]{0:T(128)} %param.29) | copy-start | bytes 1540
  0.7 53.5 %copy-start.4 = (bf16[1024,64]{0,1:T(8,128)(2,1)S(1)}, bf16[1024,64]{0,1:T(8,128)(2,1)}, u32[]{:S(2)}) copy-start(bf16[1024,64]{0,1:T(8,128)(2,1)} %param.30) | copy-start | bytes 393220
  0.7 63.8 %copy-start.8 = (f32[2048]{0:T(1024)S(1)}, f32[2048]{0:T(1024)}, u32[]{:S(2)}) copy-start(f32[2048]{0:T(1024)} %param.31) | copy-start | bytes 24580
  0.7 63.8 %copy-start.7 = (f32[2048]{0:T(1024)S(1)}, f32[2048]{0:T(1024)}, u32[]{:S(2)}) copy-start(f32[2048]{0:T(1024)} %param.32) | copy-start | bytes 24580
  24.5 44.5 %copy-start.11 = (bf16[2048]{0:T(1024)(128)(2,1)S(1)}, bf16[2048]{0:T(1024)(128)(2,1)}, u32[]{:S(2)}) copy-start(bf16[2048]{0:T(1024)(128)(2,1)} %param.34) | copy-start | bytes 12292
  24.5 44.6 %copy-start.6 = (s32[128,2]{0,1:T(2,128)S(1)}, s32[128,2]{0,1:T(2,128)}, u32[]{:S(2)}) copy-start(s32[128,2]{0,1:T(2,128)} %param.43) | copy-start | bytes 3076
  26.6 10.2 %all-to-all-start.1 = ((bf16[32,4,128]{2,1,0:T(4,128)(2,1)}), bf16[32,4,128]{2,1,0:T(4,128)(2,1)S(1)}, u32[]{:S(2)}, u32[]{:S(2)}) async-start(bf16[32,4,128]{2,1,0:T(4,128)(2,1)} %bitcast.3), calls=%async_computation.1 | async-start | bytes 65536 | tf_op jit(solution)/shard_map/all_to_all | solution.py:129
  40.5 50.5 %copy-start.1 = (f32[4,8,128,128]{3,2,1,0:T(8,128)}, f32[4,8,128,128]{3,2,1,0:T(8,128)S(1)}, u32[]{:S(2)}) copy-start(f32[4,8,128,128]{3,2,1,0:T(8,128)S(1)} %multiply_add_fusion) | copy-start | bytes 6291460
  65.6 18.9 %all-to-all-start.4 = ((bf16[32,4,2048]{2,1,0:T(4,128)(2,1)}), bf16[32,4,2048]{2,1,0:T(4,128)(2,1)}, u32[]{:S(2)}, u32[]{:S(2)}) async-start(bf16[32,4,2048]{2,1,0:T(4,128)(2,1)} %broadcast_in_dim.27), calls=%async_computation.4 | async-start | bytes 1048576 | tf_op jit(solution)/shard_map/all_to_all | solution.py:51
  85.7 5.2 %copy-start.2 = (bf16[2048,176]{0,1:T(8,128)(2,1)S(1)}, bf16[2048,176]{0,1:T(8,128)(2,1)}, u32[]{:S(2)}) copy-start(bf16[2048,176]{0,1:T(8,128)(2,1)} %param.35) | copy-start | bytes 2162692
  85.8 5.8 %copy-start.5 = (bf16[2048,8]{0,1:T(8,128)(2,1)S(1)}, bf16[2048,8]{0,1:T(8,128)(2,1)}, u32[]{:S(2)}) copy-start(bf16[2048,8]{0,1:T(8,128)(2,1)} %param.33) | copy-start | bytes 98308
  91.9 29.1 %copy-start.9 = (f32[2048]{0:T(1024)S(1)}, f32[2048]{0:T(1024)}, u32[]{:S(2)}) copy-start(f32[2048]{0:T(1024)} %param.42) | copy-start | bytes 24580
  91.9 29.1 %copy-start.10 = (f32[2048]{0:T(1024)S(1)}, f32[2048]{0:T(1024)}, u32[]{:S(2)}) copy-start(f32[2048]{0:T(1024)} %param.41) | copy-start | bytes 24580

commit v2 on v1

v2 whole, which is shorter than its diff:
```python
import jax
import jax.numpy as jnp
from jax import lax
import functools

from jax.experimental import pallas as pl
from jax.experimental.pallas import tpu as pltpu
from jax.sharding import PartitionSpec as P

EXPERTS = 8
MESH = pl.DeviceIdType.MESH


ALPHA = 8.0**0.25
NORM_EPS = 1e-05
HEAD_EPS = 1e-06


def layer_norm(mixture, gain, bias):
    center = jnp.mean(mixture, axis=-1, keepdims=True)
    spread = jnp.mean(jnp.square(mixture - center), axis=-1, keepdims=True)
    return (mixture - center) * lax.rsqrt(spread + NORM_EPS) * gain + bias


def recurrence(projected, state, lower_bound, head_gain):
    nseq, heads, width = (state.shape[0], state.shape[1], state.shape[2])
    query = projected[:, 0].astype(jnp.float32).reshape(nseq, heads, width)
    forget_in = projected[:, 1].astype(jnp.float32)
    value = projected[:, 2].astype(jnp.float32).reshape(nseq, heads, width)
    outgate = projected[:, 3].astype(jnp.float32)
    forget = (lower_bound + (1.0 - lower_bound) * jax.nn.sigmoid(forget_in)).reshape(
        nseq, heads, width
    )
    keyed = ((1.0 - lower_bound) * jax.nn.sigmoid(-forget_in)).reshape(nseq, heads, width)
    fresh = forget[..., None] * state + keyed[..., None] * value[:, :, None, :]
    read = jnp.einsum("bhkv,bhk->bhv", fresh, query, precision=lax.Precision.HIGHEST)
    scaled = (
        read * lax.rsqrt(jnp.mean(jnp.square(read), axis=-1, keepdims=True) + HEAD_EPS) * head_gain
    )
    mixed = (scaled.reshape(nseq, heads * width) * jax.nn.silu(outgate)).astype(jnp.bfloat16)
    return (mixed, fresh)


def greet(n, me):
    barrier = pltpu.get_barrier_semaphore()

    @pl.loop(1, n)
    def _(k):
        pl.semaphore_signal(
            barrier, inc=1, device_id=(lax.rem(me + k, n),), device_id_type=MESH
        )

    pl.semaphore_wait(barrier, n - 1)


def start_all(source, dest, send_sem, recv_sem, n, me):
    @pl.loop(1, n)
    def _(k):
        peer = lax.rem(me + k, n)
        pltpu.make_async_remote_copy(
            src_ref=source(peer),
            dst_ref=dest.at[me],
            send_sem=send_sem.at[k],
            recv_sem=recv_sem.at[k],
            device_id=(peer,),
            device_id_type=MESH,
        ).start()


def wait_all(source, dest, send_sem, recv_sem, n, me):
    @pl.loop(1, n)
    def _(k):
        peer = lax.rem(me + k, n)
        pltpu.make_async_remote_copy(
            src_ref=source(peer),
            dst_ref=dest.at[lax.rem(me + n - k, n)],
            send_sem=send_sem.at[k],
            recv_sem=recv_sem.at[k],
            device_id=(peer,),
            device_id_type=MESH,
        ).wait()


def flatten_rows(blocks, flat, n, nseq):
    group = max(1, 16 // nseq)

    @pl.loop(0, n // group)
    def _(i):
        parts = [blocks[i * group + j].astype(jnp.float32) for j in range(group)]
        at = pl.multiple_of(i * (group * nseq), group * nseq)
        flat[pl.ds(at, group * nseq), :] = jnp.concatenate(parts, axis=0).astype(flat.dtype)


def split_rows(flat, blocks, n, nseq):
    group = max(1, 8 // nseq)

    @pl.loop(0, n // group)
    def _(i):
        at = pl.multiple_of(i * (group * nseq), group * nseq)
        taken = flat[pl.ds(at, group * nseq), :]
        for j in range(group):
            blocks[i * group + j] = taken[j * nseq : (j + 1) * nseq].astype(blocks.dtype)


def project_kernel(
    n, block_ref, weight_hbm, out_ref,
    weight, gathered, rows, made, outgoing, landed,
    weight_sem, gather_send, gather_recv, back_send, back_recv,
):
    me = lax.axis_index("ep")
    nseq = block_ref.shape[0]
    load = pltpu.make_async_copy(weight_hbm, weight, weight_sem)
    load.start()
    greet(n, me)
    own = lambda peer: block_ref
    start_all(own, gathered, gather_send, gather_recv, n, me)
    gathered[me] = block_ref[...]
    wait_all(own, gathered, gather_send, gather_recv, n, me)
    flatten_rows(gathered, rows, n, nseq)
    load.wait()
    made[...] = jnp.dot(
        rows[...], weight[...], preferred_element_type=jnp.float32
    )
    split_rows(made, outgoing, n, nseq)
    part = lambda peer: outgoing.at[peer]
    start_all(part, landed, back_send, back_recv, n, me)
    landed[me] = outgoing[me]
    wait_all(part, landed, back_send, back_recv, n, me)
    out_ref[...] = landed[...]


def exchange_semaphores(n):
    return [pltpu.SemaphoreType.DMA((n,))] * 4


def project(block, weight, n, collective_id):
    nseq, width = block.shape
    cols = weight.shape[1]
    bf16, f32 = jnp.bfloat16, jnp.float32
    return pl.pallas_call(
        functools.partial(project_kernel, n),
        out_shape=jax.ShapeDtypeStruct((n, nseq, cols), bf16),
        in_specs=[
            pl.BlockSpec(memory_space=pltpu.VMEM),
            pl.BlockSpec(memory_space=pl.ANY),
        ],
        out_specs=pl.BlockSpec(memory_space=pltpu.VMEM),
        scratch_shapes=[
            pltpu.VMEM(weight.shape, bf16),
            pltpu.VMEM((n, nseq, width), bf16),
            pltpu.VMEM((n * nseq, width), bf16),
            pltpu.VMEM((n * nseq, cols), f32),
            pltpu.VMEM((n, nseq, cols), bf16),
            pltpu.VMEM((n, nseq, cols), bf16),
            pltpu.SemaphoreType.DMA,
            *exchange_semaphores(n),
        ],
        compiler_params=pltpu.CompilerParams(
            collective_id=collective_id, has_side_effects=True, vmem_limit_bytes=24 * 2**20
        ),
    )(block, weight)


def column_tile(cols):
    return 256 if cols % 256 == 0 else cols


def for_tiles(cols, body):
    tile = column_tile(cols)
    if tile == cols:
        body(slice(None))
    else:
        pl.loop(0, cols // tile)(lambda i: body(pl.ds(pl.multiple_of(i * tile, tile), tile)))


def channel_kernel(
    n, block_ref, pick_ref, small_ref, gain_ref, bias_ref,
    gate_hbm, up_hbm, down_hbm, dense_gate_hbm, dense_up_hbm, dense_down_hbm, out_ref,
    gate_w, up_w, down_w, dense_gate_w, dense_up_w, dense_down_w,
    gathered, rows, hidden, dense_hidden, made, outgoing, landed,
    weight_sem, gather_send, gather_recv, back_send, back_recv,
):
    f32 = jnp.float32
    me = lax.axis_index("ep")
    nseq, width = block_ref.shape
    pairs = (
        (dense_gate_hbm, dense_gate_w),
        (dense_up_hbm, dense_up_w),
        (gate_hbm, gate_w),
        (up_hbm, up_w),
        (dense_down_hbm, dense_down_w),
        (down_hbm, down_w),
    )
    loads = [
        pltpu.make_async_copy(there, here, weight_sem.at[i]) for i, (there, here) in enumerate(pairs)
    ]
    for load in loads:
        load.start()
    greet(n, me)
    own = lambda peer: block_ref
    start_all(own, gathered, gather_send, gather_recv, n, me)
    gathered[me] = block_ref[...]
    wait_all(own, gathered, gather_send, gather_recv, n, me)
    flatten_rows(gathered, rows, n, nseq)
    dot = functools.partial(jnp.dot, preferred_element_type=f32)

    small = dot(rows[...], small_ref[...])
    picks = pick_ref[...]
    logit_gap = jnp.sum(small[:, :EXPERTS] * picks[:, :EXPERTS], axis=1, keepdims=True)
    share = jax.nn.sigmoid(logit_gap)
    branch_gate = jax.nn.sigmoid(small[:, EXPERTS : EXPERTS + 1])
    on_first = picks[:, EXPERTS : EXPERTS + 1] > 0
    on_second = picks[:, EXPERTS + 1 : EXPERTS + 2] > 0
    weight = jnp.where(on_first, share, jnp.where(on_second, 1.0 - share, 0.0))

    def fill(target, gate, up):
        def body(at):
            gate_part = dot(rows[...], gate[:, at])
            up_part = dot(rows[...], up[:, at])
            target[:, at] = (jax.nn.silu(gate_part) * up_part).astype(jnp.bfloat16)

        for_tiles(target.shape[1], body)

    for load in loads[:2]:
        load.wait()
    fill(dense_hidden, dense_gate_w, dense_up_w)
    for load in loads[2:4]:
        load.wait()
    fill(hidden, gate_w, up_w)
    for load in loads[4:]:
        load.wait()

    def down(at):
        routed = dot(hidden[...], down_w[:, at])
        dense = dot(dense_hidden[...], dense_down_w[:, at])
        made[:, at] = branch_gate * dense + jnp.where(weight > 0, weight * routed, 0.0)

    for_tiles(width, down)
    split_rows(made, outgoing, n, nseq)
    part = lambda peer: outgoing.at[peer]
    start_all(part, landed, back_send, back_recv, n, me)
    landed[me] = outgoing[me]
    wait_all(part, landed, back_send, back_recv, n, me)
    channel = lax.fori_loop(
        0, n, lambda d, total: total + landed[d].astype(f32), jnp.zeros((nseq, width), f32)
    )
    mixture = ALPHA * block_ref[...].astype(f32) + channel
    out_ref[...] = layer_norm(mixture, gain_ref[...], bias_ref[...]).astype(jnp.bfloat16)


def channel_and_norm(
    normed, routes, n, router_weight, branch_vector, dense_gate_weight, dense_up_weight,
    dense_down_weight, expert_gate_weight, expert_up_weight, expert_down_weight, gain, bias,
):
    bf16, f32 = jnp.bfloat16, jnp.float32
    nseq, width = normed.shape
    total = n * nseq
    expert = lax.axis_index("ep") // (n // EXPERTS)
    first = jax.nn.one_hot(routes[:, 0], EXPERTS, dtype=f32)
    second = jax.nn.one_hot(routes[:, 1], EXPERTS, dtype=f32)
    picks = jnp.concatenate([first - second, (routes == expert).astype(f32)], axis=1)
    small = jnp.concatenate([router_weight, branch_vector[:, None]], axis=1)
    weights = (
        expert_gate_weight,
        expert_up_weight,
        expert_down_weight,
        dense_gate_weight,
        dense_up_weight,
        dense_down_weight,
    )
    vmem, anywhere = pl.BlockSpec(memory_space=pltpu.VMEM), pl.BlockSpec(memory_space=pl.ANY)
    return pl.pallas_call(
        functools.partial(channel_kernel, n),
        out_shape=jax.ShapeDtypeStruct((nseq, width), bf16),
        in_specs=[vmem] * 5 + [anywhere] * 6,
        out_specs=vmem,
        scratch_shapes=[
            *[pltpu.VMEM(w.shape, bf16) for w in weights],
            pltpu.VMEM((n, nseq, width), bf16),
            pltpu.VMEM((total, width), bf16),
            pltpu.VMEM((total, expert_gate_weight.shape[1]), bf16),
            pltpu.VMEM((total, dense_gate_weight.shape[1]), bf16),
            pltpu.VMEM((total, width), f32),
            pltpu.VMEM((n, nseq, width), bf16),
            pltpu.VMEM((n, nseq, width), bf16),
            pltpu.SemaphoreType.DMA((6,)),
            *exchange_semaphores(n),
        ],
        compiler_params=pltpu.CompilerParams(
            collective_id=2, has_side_effects=True, vmem_limit_bytes=56 * 2**20
        ),
    )(normed, picks, small, gain[None], bias[None], *weights)


def per_device(
    tokens,
    recurrent_state,
    query_weight,
    forget_weight,
    input_weight,
    outgate_weight,
    lower_bound,
    head_gain,
    mixout_weight,
    first_gain,
    first_bias,
    router_weight,
    branch_vector,
    dense_gate_weight,
    dense_up_weight,
    dense_down_weight,
    expert_gate_weight,
    expert_up_weight,
    expert_down_weight,
    second_gain,
    second_bias,
    routes,
):
    f32 = jnp.float32
    devices = lax.axis_size("ep")
    nseq, width = tokens.shape
    own_cols = query_weight.shape[1]
    stacked = jnp.concatenate([query_weight, forget_weight, input_weight, outgate_weight], axis=1)
    owned = project(tokens, stacked, devices, 0)
    projected = (
        owned.reshape(devices, nseq, 4, own_cols)
        .transpose(1, 2, 0, 3)
        .reshape(nseq, 4, devices * own_cols)
    )
    mixed, new_state = recurrence(projected, recurrent_state, lower_bound, head_gain)
    mix_out = project(mixed, mixout_weight, devices, 1).transpose(1, 0, 2).reshape(nseq, width)
    normed = layer_norm(
        ALPHA * tokens.astype(f32) + mix_out.astype(f32), first_gain, first_bias
    ).astype(jnp.bfloat16)
    output = channel_and_norm(
        normed,
        routes,
        devices,
        router_weight,
        branch_vector,
        dense_gate_weight,
        dense_up_weight,
        dense_down_weight,
        expert_gate_weight,
        expert_up_weight,
        expert_down_weight,
        second_gain,
        second_bias,
    )
    return (output, new_state)


def solution(mesh):
    return jax.shard_map(
        per_device,
        mesh=mesh,
        in_specs=(
            P("ep", None),
            P("ep", None, None, None),
            P(None, "ep"),
            P(None, "ep"),
            P(None, "ep"),
            P(None, "ep"),
            P(),
            P(),
            P(None, "ep"),
            P(),
            P(),
            P(),
            P(),
            P(None, "ep"),
            P(None, "ep"),
            P("ep", None),
            P(None, "ep"),
            P(None, "ep"),
            P("ep", None),
            P(),
            P(),
            P(),
        ),
        out_specs=(P("ep", None), P("ep", None, None, None)),
        check_vma=False,
    )
```

time: 122 us -> 99.6 us (0.82)
  the two profiles are of different devices: /device:TPU:0 before, /device:TPU:29 now
where the time goes in v2:
time: 99.6 us; the launch traced here: 99.3 us
  Pallas kernels  81.7 us (82%)
  local copies, waits for them, and re-layouts  11.1 us (11%)
  other arithmetic  4.48 us (4%)
  matrix products  1.06 us (1%)
    pallas_call x1, Pallas kernels, channel_and_norm(): pl.pallas_call(functools.partial(channel_kernel, n), out_shape=jax.ShapeD...  41.1 us
    pallas_call x2, Pallas kernels, project(): pl.pallas_call(functools.partial(project_kernel, n), out_shape=jax.ShapeD...  40.6 us
    unnamed x33, local copies, waits for them, and re-layouts  8.88 us
    add x1, other arithmetic, recurrence(): fresh = forget[..., None] * state + keyed[..., None] * value[:, :, None, :]  2.47 us

profile of v2, /device:TPU:29, one launch (start us, length us, event | category | flops | bytes accessed | tf_op | source)
XLA Modules:
  0.0 99.3 jit_solution(4640186636518062213)
XLA Ops:
  0.6 1.2 %copy.52 = bf16[2048,32]{1,0:T(8,128)(2,1)S(1)} copy(bf16[2048,32]{0,1:T(8,128)(2,1)} %param.27) | data formatting | bytes 262144 | tf_op args[5]
  1.8 1.2 %copy.51 = bf16[2048,32]{1,0:T(8,128)(2,1)S(1)} copy(bf16[2048,32]{0,1:T(8,128)(2,1)} %param.26) | data formatting | bytes 262144 | tf_op args[4]
  3.0 1.2 %copy.50 = bf16[2048,32]{1,0:T(8,128)(2,1)S(1)} copy(bf16[2048,32]{0,1:T(8,128)(2,1)} %param.25) | data formatting | bytes 262144 | tf_op args[3]
  4.2 1.2 %copy.49 = bf16[2048,32]{1,0:T(8,128)(2,1)S(1)} copy(bf16[2048,32]{0,1:T(8,128)(2,1)} %param.24) | data formatting | bytes 262144 | tf_op args[2]
  5.4 0.7 pad_maximum_fusion.weight_hbm
  6.1 22.7 %shard_map.221 = bf16[32,4,128]{2,1,0:T(4,128)(2,1)S(1)} custom-call(bf16[4,2048]{1,0:T(4,128)(2,1)S(1)} %copy-done, bf16[2048,128]{1,0:T(8,128)(2,1)S(1)} %pad_maximum_fusion.weight_hbm), custom_call_target="tpu_custom_call" | custom-call | tf_op jit(solution)/shard_map/pallas_call | solution.py:140
  28.8 0.1 reshape.102
  29.0 0.2 reshape.103
  29.3 2.5 %multiply_add_fusion = f32[4,8,128,128]{3,2,1,0:T(8,128)S(1)} fusion(f32[4,8,128,128]{3,2,1,0:T(8,128)} %param.23, f32[4,8,128]{2,1,0:T(8,128)S(1)} %bitcast.59, f32[4,8,128]{2,1,0:T(8,128)S(1)} %get-tuple-element.7, f32[4,8,128]{2,1,0:T(8,128)S(1)} %get-tuple-element.6), kind=kLoop, calls=%fused_computation | loop fusion | flops 1572864 | bytes 4243456 | tf_op jit(solution)/shard_map/add | solution.py:35
  31.9 1.1 %fusion.14 = f32[4,8,1,128]{3,2,1,0:T(1,128)S(1)} fusion(f32[4,8,128,128]{3,2,1,0:T(8,128)S(1)} %multiply_add_fusion, bf16[4,8,128,1]{2,3,1,0:T(2,128)(2,1)S(1)} %reshape.114), kind=kOutput, calls=%fused_computation.44 | convolution fusion | flops 6291456 | bytes 2121728 | tf_op jit(solution)/shard_map/bhkv,bhk->bhv/dot_general | solution.py:36
  33.0 0.1 multiply_reduce_fusion.1
  33.1 0.1 multiply_bitcast_fusion
  33.2 0.2 copy.54.weight_hbm
  33.4 17.8 %shard_map.222 = bf16[32,4,64]{2,1,0:T(4,128)(2,1)S(1)} custom-call(bf16[4,1024]{1,0:T(4,128)(2,1)S(1)} %fusion.11.block_ref, bf16[1024,64]{1,0:T(8,128)(2,1)S(1)} %copy.54.weight_hbm), custom_call_target="tpu_custom_call" | custom-call | tf_op jit(solution)/shard_map/pallas_call | solution.py:140
  51.2 0.1 reshape.110
  51.3 0.1 fusion.12
  51.5 0.2 multiply_reduce_fusion
  51.7 0.7 add_convert_fusion.block_ref
  52.4 0.7 copy.56.pick_ref
  53.2 1.0 %copy.57.small_ref = bf16[2048,9]{1,0:T(8,128)(2,1)} copy(bf16[2048,9]{0,1:T(8,128)(2,1)S(1)} %pad_maximum_fusion.1) | data formatting | bytes 73728 | tf_op jit(solution)/shard_map/concatenate | solution.py:262
  54.2 1.3 %copy.58.dense_gate_hbm = bf16[2048,176]{1,0:T(8,128)(2,1)} copy(bf16[2048,176]{0,1:T(8,128)(2,1)S(1)} %copy-done.2) | data formatting | bytes 1441792 | tf_op args[13]
  55.5 1.3 %copy.59.dense_up_hbm = bf16[2048,176]{1,0:T(8,128)(2,1)} copy(bf16[2048,176]{0,1:T(8,128)(2,1)S(1)} %copy-done.3) | data formatting | bytes 1441792 | tf_op args[14]
  56.8 41.1 %shard_map.223 = bf16[4,2048]{1,0:T(4,128)(2,1)} custom-call(bf16[4,2048]{1,0:T(4,128)(2,1)} %add_convert_fusion.block_ref, f32[128,10]{1,0:T(8,128)} %copy.56.pick_ref, bf16[2048,9]{1,0:T(8,128)(2,1)} %copy.57.small_ref, f32[1,2048]{1,0:T(1,128)} %bitcast.61, f32[1,2048]{1,0:T(1,128)} %bitcast.62, bf16[2048,1792]{1,0:T(8,128)(2,1)} %gate_hbm.1, ...), custom_call_target="tpu_custom_call" | custom-call | tf_op jit(solution)/shard_map/pallas_call | solution.py:272
  98.0 1.3 %copy.76 = bf16[4,2048]{1,0:T(4,128)(2,1)} copy(bf16[4,2048]{1,0:T(4,128)(2,1)} %shard_map.223) | data formatting | bytes 32768
  (43 shorter events, 0.3 us)
Async XLA Ops:
  3.0 3.1 %copy-start = (bf16[4,2048]{1,0:T(4,128)(2,1)S(1)}, bf16[4,2048]{1,0:T(4,128)(2,1)}, u32[]{:S(2)}) copy-start(bf16[4,2048]{1,0:T(4,128)(2,1)} %block_ref.1) | copy-start | bytes 49156
  5.4 23.9 %copy-start.6 = (f32[1024]{0:T(1024)S(1)}, f32[1024]{0:T(1024)}, u32[]{:S(2)}) copy-start(f32[1024]{0:T(1024)} %param.28) | copy-start | bytes 12292
  31.8 22.5 %copy-start.1 = (f32[4,8,128,128]{3,2,1,0:T(8,128)}, f32[4,8,128,128]{3,2,1,0:T(8,128)S(1)}, u32[]{:S(2)}) copy-start(f32[4,8,128,128]{3,2,1,0:T(8,128)S(1)} %multiply_add_fusion) | copy-start | bytes 6291460
  31.8 1.3 %copy-start.11 = (f32[128]{0:T(128)S(1)}, f32[128]{0:T(128)}, u32[]{:S(2)}) copy-start(f32[128]{0:T(128)} %param.29) | copy-start | bytes 1540
  31.8 1.4 %copy-start.4 = (bf16[1024,64]{0,1:T(8,128)(2,1)S(1)}, bf16[1024,64]{0,1:T(8,128)(2,1)}, u32[]{:S(2)}) copy-start(bf16[1024,64]{0,1:T(8,128)(2,1)} %param.30) | copy-start | bytes 393220
  31.8 19.9 %copy-start.7 = (f32[2048]{0:T(1024)S(1)}, f32[2048]{0:T(1024)}, u32[]{:S(2)}) copy-start(f32[2048]{0:T(1024)} %param.32) | copy-start | bytes 24580
  31.8 19.9 %copy-start.8 = (f32[2048]{0:T(1024)S(1)}, f32[2048]{0:T(1024)}, u32[]{:S(2)}) copy-start(f32[2048]{0:T(1024)} %param.31) | copy-start | bytes 24580
  31.8 20.6 %copy-start.10 = (s32[128,2]{0,1:T(2,128)S(1)}, s32[128,2]{0,1:T(2,128)}, u32[]{:S(2)}) copy-start(s32[128,2]{0,1:T(2,128)} %param.43) | copy-start | bytes 3076
  31.8 21.3 %copy-start.9 = (bf16[2048]{0:T(1024)(128)(2,1)S(1)}, bf16[2048]{0:T(1024)(128)(2,1)}, u32[]{:S(2)}) copy-start(bf16[2048]{0:T(1024)(128)(2,1)} %param.34) | copy-start | bytes 12292
  31.8 21.3 %copy-start.5 = (bf16[2048,8]{0,1:T(8,128)(2,1)S(1)}, bf16[2048,8]{0,1:T(8,128)(2,1)}, u32[]{:S(2)}) copy-start(bf16[2048,8]{0,1:T(8,128)(2,1)} %param.33) | copy-start | bytes 98308
  31.9 22.4 %copy-start.2 = (bf16[2048,176]{0,1:T(8,128)(2,1)S(1)}, bf16[2048,176]{0,1:T(8,128)(2,1)}, u32[]{:S(2)}) copy-start(bf16[2048,176]{0,1:T(8,128)(2,1)} %param.35) | copy-start | bytes 2162692
  54.2 1.3 %copy-start.3 = (bf16[2048,176]{0,1:T(8,128)(2,1)S(1)}, bf16[2048,176]{0,1:T(8,128)(2,1)}, u32[]{:S(2)}) copy-start(bf16[2048,176]{0,1:T(8,128)(2,1)} %param.36) | copy-start | bytes 2162692

commit v3 on v2

--- a/solution.py
+++ b/solution.py
@@ -81,6 +81,55 @@
         ).wait()
 
 
+def gather_all(block_ref, gathered, send_sem, recv_sem, n, me):
+    chips = n // 2
+    chip, core = lax.div(me, 2), lax.rem(me, 2)
+    sibling = 2 * chip + 1 - core
+
+    def across(k, owner):
+        return pltpu.make_async_remote_copy(
+            src_ref=block_ref,
+            dst_ref=gathered.at[owner],
+            send_sem=send_sem.at[k],
+            recv_sem=recv_sem.at[k],
+            device_id=(2 * lax.rem(chip + k, chips) + core,),
+            device_id_type=MESH,
+        )
+
+    def onward(k, source, owner):
+        return pltpu.make_async_remote_copy(
+            src_ref=source,
+            dst_ref=gathered.at[owner],
+            send_sem=send_sem.at[chips + k],
+            recv_sem=recv_sem.at[chips + k],
+            device_id=(sibling,),
+            device_id_type=MESH,
+        )
+
+    pl.loop(1, chips)(lambda k: across(k, me).start())
+    onward(0, block_ref, me).start()
+    gathered[me] = block_ref[...]
+
+    @pl.loop(1, chips)
+    def _(k):
+        owner = 2 * lax.rem(chip + chips - k, chips) + core
+        across(k, owner).wait()
+        onward(k, gathered.at[owner], owner).start()
+
+    onward(0, block_ref, sibling).wait()
+
+    @pl.loop(1, chips)
+    def _(k):
+        base = 2 * lax.rem(chip + chips - k, chips)
+        onward(k, gathered.at[base + core], base + 1 - core).wait()
+
+
+def dot_turned(rows, weight):
+    return lax.dot_general(
+        rows, weight, (((1,), (1,)), ((), ())), preferred_element_type=jnp.float32
+    )
+
+
 def flatten_rows(blocks, flat, n, nseq):
     group = max(1, 16 // nseq)
 
@@ -112,15 +161,10 @@
     load = pltpu.make_async_copy(weight_hbm, weight, weight_sem)
     load.start()
     greet(n, me)
-    own = lambda peer: block_ref
-    start_all(own, gathered, gather_send, gather_recv, n, me)
-    gathered[me] = block_ref[...]
-    wait_all(own, gathered, gather_send, gather_recv, n, me)
+    gather_all(block_ref, gathered, gather_send, gather_recv, n, me)
     flatten_rows(gathered, rows, n, nseq)
     load.wait()
-    made[...] = jnp.dot(
-        rows[...], weight[...], preferred_element_type=jnp.float32
-    )
+    made[...] = dot_turned(rows[...], weight[...])
     split_rows(made, outgoing, n, nseq)
     part = lambda peer: outgoing.at[peer]
     start_all(part, landed, back_send, back_recv, n, me)
@@ -135,7 +179,7 @@
 
 def project(block, weight, n, collective_id):
     nseq, width = block.shape
-    cols = weight.shape[1]
+    cols = weight.shape[0]
     bf16, f32 = jnp.bfloat16, jnp.float32
     return pl.pallas_call(
         functools.partial(project_kernel, n),
@@ -197,14 +241,11 @@
     for load in loads:
         load.start()
     greet(n, me)
-    own = lambda peer: block_ref
-    start_all(own, gathered, gather_send, gather_recv, n, me)
-    gathered[me] = block_ref[...]
-    wait_all(own, gathered, gather_send, gather_recv, n, me)
+    gather_all(block_ref, gathered, gather_send, gather_recv, n, me)
     flatten_rows(gathered, rows, n, nseq)
     dot = functools.partial(jnp.dot, preferred_element_type=f32)
 
-    small = dot(rows[...], small_ref[...])
+    small = dot_turned(rows[...], small_ref[...])
     picks = pick_ref[...]
     logit_gap = jnp.sum(small[:, :EXPERTS] * picks[:, :EXPERTS], axis=1, keepdims=True)
     share = jax.nn.sigmoid(logit_gap)
@@ -223,7 +264,9 @@
 
     for load in loads[:2]:
         load.wait()
-    fill(dense_hidden, dense_gate_w, dense_up_w)
+    gate_part = dot_turned(rows[...], dense_gate_w[...])
+    up_part = dot_turned(rows[...], dense_up_w[...])
+    dense_hidden[...] = (jax.nn.silu(gate_part) * up_part).astype(jnp.bfloat16)
     for load in loads[2:4]:
         load.wait()
     fill(hidden, gate_w, up_w)
@@ -259,13 +302,13 @@
     first = jax.nn.one_hot(routes[:, 0], EXPERTS, dtype=f32)
     second = jax.nn.one_hot(routes[:, 1], EXPERTS, dtype=f32)
     picks = jnp.concatenate([first - second, (routes == expert).astype(f32)], axis=1)
-    small = jnp.concatenate([router_weight, branch_vector[:, None]], axis=1)
+    small = jnp.concatenate([router_weight.T, branch_vector[None]], axis=0)
     weights = (
         expert_gate_weight,
         expert_up_weight,
         expert_down_weight,
-        dense_gate_weight,
-        dense_up_weight,
+        dense_gate_weight.T,
+        dense_up_weight.T,
         dense_down_weight,
     )
     vmem, anywhere = pl.BlockSpec(memory_space=pltpu.VMEM), pl.BlockSpec(memory_space=pl.ANY)
@@ -320,7 +363,9 @@
     devices = lax.axis_size("ep")
     nseq, width = tokens.shape
     own_cols = query_weight.shape[1]
-    stacked = jnp.concatenate([query_weight, forget_weight, input_weight, outgate_weight], axis=1)
+    stacked = jnp.concatenate(
+        [query_weight.T, forget_weight.T, input_weight.T, outgate_weight.T], axis=0
+    )
     owned = project(tokens, stacked, devices, 0)
     projected = (
         owned.reshape(devices, nseq, 4, own_cols)
@@ -328,7 +373,7 @@
         .reshape(nseq, 4, devices * own_cols)
     )
     mixed, new_state = recurrence(projected, recurrent_state, lower_bound, head_gain)
-    mix_out = project(mixed, mixout_weight, devices, 1).transpose(1, 0, 2).reshape(nseq, width)
+    mix_out = project(mixed, mixout_weight.T, devices, 1).transpose(1, 0, 2).reshape(nseq, width)
     normed = layer_norm(
         ALPHA * tokens.astype(f32) + mix_out.astype(f32), first_gain, first_bias
     ).astype(jnp.bfloat16)

time: 99.6 us -> 82 us (0.82)
  Pallas kernels: 81.7 us -> 70.8 us
  local copies, waits for them, and re-layouts: 11.1 us -> 3.29 us
  other arithmetic: 4.48 us -> 5.57 us
    unnamed x33 -> x24, local copies, waits for them, and re-layouts: 8.88 us -> 2.11 us
    pallas_call x2, Pallas kernels: 40.6 us -> 34.4 us  [project(): pl.pallas_call(functools.partial(project_kernel, n), out_shape=jax.ShapeD...]
    pallas_call x1, Pallas kernels: 41.1 us -> 36.5 us  [channel_and_norm(): pl.pallas_call(functools.partial(channel_kernel, n), out_shape=jax.ShapeD...]
    concatenate x2, other arithmetic: 0.7 us -> 1.78 us  [the longest x1 1.14 us: per_device(): jnp.concatenate([query_weight.T, forget_weight.T, input_weight.T, outgate...]
    concatenate x1 -> x0, local copies, waits for them, and re-layouts: 1.05 us -> none  [channel_and_norm(): small = jnp.concatenate([router_weight, branch_vector[:, None]], axis=1)]
where the time goes in v3:
time: 82 us; the launch traced here: 81.7 us
  Pallas kernels  70.8 us (86%)
  other arithmetic  5.57 us (7%)
  local copies, waits for them, and re-layouts  3.29 us (4%)
  matrix products  1.06 us (1%)
  between operations  0.92 us (1%)
    pallas_call x1, Pallas kernels, channel_and_norm(): pl.pallas_call(functools.partial(channel_kernel, n), out_shape=jax.ShapeD...  36.5 us
    pallas_call x2, Pallas kernels, project(): pl.pallas_call(functools.partial(project_kernel, n), out_shape=jax.ShapeD...  34.4 us
    add x1, other arithmetic, recurrence(): fresh = forget[..., None] * state + keyed[..., None] * value[:, :, None, :]  2.48 us
    unnamed x24, local copies, waits for them, and re-layouts  2.11 us

profile of v3, /device:TPU:29, one launch (start us, length us, event | category | flops | bytes accessed | tf_op | source)
XLA Modules:
  0.0 81.7 jit_solution(12608013460540657157)
XLA Ops:
  0.6 1.1 %pad_maximum_fusion.weight_hbm = bf16[128,2048]{1,0:T(8,128)(2,1)S(1)} fusion(bf16[32,2048]{1,0:T(8,128)(2,1)} %bitcast.70, bf16[32,2048]{1,0:T(8,128)(2,1)} %bitcast.71, bf16[32,2048]{1,0:T(8,128)(2,1)} %bitcast.72, bf16[32,2048]{1,0:T(8,128)(2,1)} %bitcast.73), kind=kLoop, calls=%fused_computation.1 | loop fusion | flops 2097152 | bytes 1048576 | tf_op jit(solution)/shard_map/concatenate | solution.py:366
  1.8 0.0 copy-start
  1.8 0.7 copy-done
  2.5 17.8 %shard_map.221 = bf16[32,4,128]{2,1,0:T(4,128)(2,1)S(1)} custom-call(bf16[4,2048]{1,0:T(4,128)(2,1)S(1)} %copy-done, bf16[128,2048]{1,0:T(8,128)(2,1)S(1)} %pad_maximum_fusion.weight_hbm), custom_call_target="tpu_custom_call" | custom-call | tf_op jit(solution)/shard_map/pallas_call | solution.py:184
  20.3 0.1 reshape.102
  20.5 0.2 reshape.103
  20.8 2.5 %multiply_add_fusion = f32[4,8,128,128]{3,2,1,0:T(8,128)S(1)} fusion(f32[4,8,128,128]{3,2,1,0:T(8,128)} %param.23, f32[4,8,128]{2,1,0:T(8,128)S(1)} %bitcast.74, f32[4,8,128]{2,1,0:T(8,128)S(1)} %get-tuple-element.7, f32[4,8,128]{2,1,0:T(8,128)S(1)} %get-tuple-element.6), kind=kLoop, calls=%fused_computation | loop fusion | flops 1572864 | bytes 4243456 | tf_op jit(solution)/shard_map/add | solution.py:35
  23.2 0.0 copy-start.3
  23.3 0.0 copy-start.10
  23.3 0.0 copy-start.2
  23.3 0.0 copy-start.7
  23.3 0.0 copy-start.9
  23.4 1.1 %fusion.14 = f32[4,8,1,128]{3,2,1,0:T(1,128)S(1)} fusion(f32[4,8,128,128]{3,2,1,0:T(8,128)S(1)} %multiply_add_fusion, bf16[4,8,128,1]{2,3,1,0:T(2,128)(2,1)S(1)} %reshape.114), kind=kOutput, calls=%fused_computation.44 | convolution fusion | flops 6291456 | bytes 2121728 | tf_op jit(solution)/shard_map/bhkv,bhk->bhv/dot_general | solution.py:36
  24.4 0.1 multiply_reduce_fusion.1
  24.5 0.1 multiply_bitcast_fusion
  24.7 16.6 %shard_map.222 = bf16[32,4,64]{2,1,0:T(4,128)(2,1)S(1)} custom-call(bf16[4,1024]{1,0:T(4,128)(2,1)S(1)} %fusion.11.block_ref, bf16[64,1024]{1,0:T(8,128)(2,1)S(1)} %bitcast.64), custom_call_target="tpu_custom_call" | custom-call | tf_op jit(solution)/shard_map/pallas_call | solution.py:184
  41.3 0.1 reshape.110
  41.4 0.1 fusion.12
  41.5 0.2 multiply_reduce_fusion
  41.7 0.7 add_convert_fusion.block_ref
  42.5 0.7 copy.30.pick_ref
  43.2 0.6 pad_maximum_fusion.1.small_ref
  43.9 36.5 %shard_map.223 = bf16[4,2048]{1,0:T(4,128)(2,1)} custom-call(bf16[4,2048]{1,0:T(4,128)(2,1)} %add_convert_fusion.block_ref, f32[128,10]{1,0:T(8,128)} %copy.30.pick_ref, bf16[9,2048]{1,0:T(8,128)(2,1)} %pad_maximum_fusion.1.small_ref, f32[1,2048]{1,0:T(1,128)} %bitcast.77, f32[1,2048]{1,0:T(1,128)} %bitcast.78, bf16[2048,1792]{1,0:T(8,128)(2,1)} %gate_hbm.1, ...), custom_call_target="tpu_custom_call" | custom-call | tf_op jit(solution)/shard_map/pallas_call | solution.py:315
  80.4 1.3 %copy.47 = bf16[4,2048]{1,0:T(4,128)(2,1)} copy(bf16[4,2048]{1,0:T(4,128)(2,1)} %shard_map.223) | data formatting | bytes 32768
  (33 shorter events, 0.2 us)
Async XLA Ops:
  0.6 20.1 %copy-start.5 = (f32[1024]{0:T(1024)S(1)}, f32[1024]{0:T(1024)}, u32[]{:S(2)}) copy-start(f32[1024]{0:T(1024)} %param.28) | copy-start | bytes 12292
  1.8 0.7 copy-start
  23.2 57.1 %copy-start.3 = (f32[4,8,128,128]{3,2,1,0:T(8,128)}, f32[4,8,128,128]{3,2,1,0:T(8,128)S(1)}, u32[]{:S(2)}) copy-start(f32[4,8,128,128]{3,2,1,0:T(8,128)S(1)} %multiply_add_fusion) | copy-start | bytes 6291460
  23.3 1.3 %copy-start.10 = (f32[128]{0:T(128)S(1)}, f32[128]{0:T(128)}, u32[]{:S(2)}) copy-start(f32[128]{0:T(128)} %param.29) | copy-start | bytes 1540
  23.3 1.4 %copy-start.2 = (bf16[1024,64]{0,1:T(8,128)(2,1)S(1)}, bf16[1024,64]{0,1:T(8,128)(2,1)}, u32[]{:S(2)}) copy-start(bf16[1024,64]{0,1:T(8,128)(2,1)} %param.30) | copy-start | bytes 393220
  23.3 18.1 %copy-start.1 = (bf16[4,2048]{1,0:T(4,128)(2,1)S(1)}, bf16[4,2048]{1,0:T(4,128)(2,1)}, u32[]{:S(2)}) copy-start(bf16[4,2048]{1,0:T(4,128)(2,1)} %block_ref.1) | copy-start | bytes 49156
  23.3 18.4 %copy-start.6 = (f32[2048]{0:T(1024)S(1)}, f32[2048]{0:T(1024)}, u32[]{:S(2)}) copy-start(f32[2048]{0:T(1024)} %param.32) | copy-start | bytes 24580
  23.3 18.4 %copy-start.7 = (f32[2048]{0:T(1024)S(1)}, f32[2048]{0:T(1024)}, u32[]{:S(2)}) copy-start(f32[2048]{0:T(1024)} %param.31) | copy-start | bytes 24580
  23.3 19.1 %copy-start.9 = (s32[128,2]{0,1:T(2,128)S(1)}, s32[128,2]{0,1:T(2,128)}, u32[]{:S(2)}) copy-start(s32[128,2]{0,1:T(2,128)} %param.43) | copy-start | bytes 3076
  23.3 19.9 %copy-start.8 = (bf16[2048]{0:T(1024)(128)(2,1)S(1)}, bf16[2048]{0:T(1024)(128)(2,1)}, u32[]{:S(2)}) copy-start(bf16[2048]{0:T(1024)(128)(2,1)} %param.34) | copy-start | bytes 12292
  23.3 19.9 %copy-start.4 = (bf16[2048,8]{0,1:T(8,128)(2,1)S(1)}, bf16[2048,8]{0,1:T(8,128)(2,1)}, u32[]{:S(2)}) copy-start(bf16[2048,8]{0,1:T(8,128)(2,1)} %param.33) | copy-start | bytes 98308
